TPU v7x, 32 devices: a whole 2x2x4 slice. The times are simulated.
32 devices in a mesh: gr: 2 (over x), fs: 8 (over z, y), tp: 2 (over core).
Axes of the slice: x: 2, y: 2, z: 4, core: 2. Of those that a mesh axis runs over, the one named last changes fastest.
Arguments:
- tokens: bfloat16 [2048, 2048], P(('gr', 'tp')), may hold values from -6 to 6
- norm_gain: float32 [2048], P('fs'), may hold values from 0.1 to 1.9
- up_weight: float32 [2048, 8192], P('fs', ('gr', 'tp')), may hold values from -0.125 to 0.125
- down_weight: float32 [8192, 2048], P('fs', ('gr', 'tp')), may hold values from -0.09375 to 0.09375
Outputs:
- sampler_up: bfloat16 [2048, 8192], P(None, 'fs')
- sampler_down: bfloat16 [8192, 2048], P('fs')
- mixed: bfloat16 [2048, 2048], P(('gr', 'tp'), 'fs')
All inputs are finite; a program needn't handle non-finite values.
Results may differ from a plain program's by a relative error of at most 0.023.
Values may be sent and summed in bfloat16 or wider, within the bound.
A program may use at most 64 MiB of HBM per device.

v0:
```python
import jax
import jax.numpy as jnp
from jax import lax
from jax.sharding import PartitionSpec as P


def per_device(tokens, norm_gain, up_weight, down_weight):
    up_scaled = (norm_gain[:, None] * up_weight).astype(jnp.bfloat16)
    down_half = down_weight.astype(jnp.bfloat16)
    up_columns, down_columns = (
        lax.all_gather(up_scaled, ("gr", "tp"), axis=1, tiled=True),
        lax.all_gather(down_half, ("gr", "tp"), axis=1, tiled=True),
    )
    up_block = lax.all_to_all(up_columns, "fs", split_axis=1, concat_axis=0, tiled=True)
    widened = tokens.astype(jnp.float32)
    normed = (
        widened * lax.rsqrt(jnp.mean(widened * widened, axis=-1, keepdims=True) + 1e-06)
    ).astype(jnp.bfloat16)
    preact = jnp.dot(normed, up_block, preferred_element_type=jnp.float32)
    hidden = jnp.square(jax.nn.relu(preact)).astype(jnp.bfloat16)
    summed = lax.psum_scatter(
        lax.dot_general(
            down_columns, hidden, (((0,), (1,)), ((), ())), preferred_element_type=jnp.float32
        ).astype(jnp.bfloat16),
        "fs",
        scatter_dimension=0,
        tiled=True,
    )
    mixed = summed.T
    return (up_block, down_columns, mixed)


def solution(mesh):
    in_specs = (P(("gr", "tp"), None), P("fs"), P("fs", ("gr", "tp")), P("fs", ("gr", "tp")))
    out_specs = (P(None, "fs"), P("fs", None), P(("gr", "tp"), "fs"))
    return jax.shard_map(
        per_device, mesh=mesh, in_specs=in_specs, out_specs=out_specs, check_vma=False
    )
```

profile of v0, /device:TPU:0, one launch (start us, length us, event | category | flops | bytes accessed | tf_op | source)
XLA Modules:
  0.0 242.2 jit_solution(8741351901346556773)
XLA Ops:
  7.2 0.0 all-gather.3.cloned.1.call-start
  7.2 2.7 %multiply_convert_fusion.1 = bf16[256,2048]{1,0:T(8,128)(2,1)} fusion(f32[256,2048]{1,0:T(8,128)} %param.6, f32[256]{0:T(256)} %param.5), kind=kLoop, calls=%fused_computation.10 | loop fusion | flops 1048576 | bytes 3146752 | tf_op jit(solution)/shard_map/convert_element_type | solution.py:8
  10.0 0.0 all-gather.3.cloned.1.call-update
  10.0 37.3 %all-gather.3.cloned.1.call-done = bf16[256,8192]{1,0:T(8,128)(2,1)} async-done(((bf16[256,2048]{1,0:T(8,128)(2,1)}), bf16[256,8192]{1,0:T(8,128)(2,1)}) %all-gather.3.cloned.1.call-update) | async-done | bytes 4194320 | tf_op jit(solution)/shard_map/all_gather | solution.py:11
  47.3 4.8 %copy.10 = bf16[32,8,8,1024]{3,2,0,1:T(8,128)(2,1)} copy(bf16[32,8,8,1024]{3,2,1,0:T(8,128)(2,1)} %bitcast.13) | data formatting | bytes 8388608 | tf_op jit(solution)/shard_map/all_to_all | solution.py:14
  52.1 0.0 copy-start.1
  52.1 5.6 %all-to-all-start = ((bf16[256,8,1024]{2,0,1:T(8,128)(2,1)}), bf16[256,8,1024]{2,0,1:T(8,128)(2,1)}, u32[]{:S(2)}, u32[]{:S(2)}) async-start(bf16[256,8,1024]{2,0,1:T(8,128)(2,1)} %bitcast.12), calls=%async_computation | async-start | bytes 8388608 | tf_op jit(solution)/shard_map/all_to_all | solution.py:14
  57.8 0.0 all-gather.5.cloned.1.call-start
  57.8 0.0 copy-done.1
  57.9 1.1 convert_element_type.22
  59.0 0.0 all-gather.5.cloned.1.call-update
  59.0 0.0 reduce-scatter.2.cloned.1.call-start
  59.0 2.1 fusion
  61.1 34.6 %all-gather.5.cloned.1.call-done = bf16[1024,2048]{1,0:T(8,128)(2,1)} async-done(((bf16[1024,512]{1,0:T(8,128)(2,1)}), bf16[1024,2048]{1,0:T(8,128)(2,1)}) %all-gather.5.cloned.1.call-update) | async-done | bytes 4194320 | tf_op jit(solution)/shard_map/all_gather | solution.py:12
  95.7 55.8 %all-to-all-done = bf16[256,8,1024]{2,0,1:T(8,128)(2,1)} async-done(((bf16[256,8,1024]{2,0,1:T(8,128)(2,1)}), bf16[256,8,1024]{2,0,1:T(8,128)(2,1)}, u32[]{:S(2)}, u32[]{:S(2)}) %all-to-all-start) | async-done | bytes 4194336 | tf_op jit(solution)/shard_map/all_to_all | solution.py:14
  151.5 9.9 %fusion.2 = bf16[2048,512]{0,1:T(8,128)(2,1)} fusion(bf16[1024,2048]{1,0:T(8,128)(2,1)} %all-gather.5.cloned.1.call-done, bf16[2048,1024]{1,0:T(8,128)(2,1)} %bitcast.1, bf16[512,2048]{1,0:T(8,128)(2,1)} %param.4, f32[512]{0:T(512)S(1)} %add_rsqrt_fusion), kind=kOutput, calls=%fused_computation.6 | convolution fusion | flops 4300734464 | bytes 12584960 | tf_op jit(solution)/shard_map/dot_general | solution.py:22
  161.4 0.0 reduce-scatter.2.cloned.1.call-update
  161.4 67.4 %reduce-scatter.2.cloned.1.call-done = bf16[256,512]{0,1:T(8,128)(2,1)} async-done(((bf16[2048,512]{0,1:T(8,128)(2,1)}), bf16[256,512]{0,1:T(8,128)(2,1)}) %reduce-scatter.2.cloned.1.call-update) | async-done | bytes 262160 | tf_op jit(solution)/shard_map/reduce_scatter | solution.py:21
  228.8 0.0 copy-start
  228.8 4.8 %copy.13 = bf16[2048,1024]{1,0:T(8,128)(2,1)} copy(bf16[2048,1024]{1,0:T(8,128)(2,1)} %bitcast.1) | data formatting | bytes 8388608
  233.7 0.0 copy-done
  233.7 2.0 copy.14
  (1 shorter events, 0.0 us)
Async XLA Ops:
  7.2 40.2 %all-gather.3.cloned.1.call-start = ((), (), s32[]{:S(2)}) async-start(), calls=%async_computation.2 | async-start | bytes 5242880 | tf_op jit(solution)/shard_map/all_gather | solution.py:11
  52.1 5.7 %copy-start.1 = (f32[1024,512]{1,0:T(8,128)S(1)}, f32[1024,512]{1,0:T(8,128)}, u32[]{:S(2)}) copy-start(f32[1024,512]{1,0:T(8,128)} %param.7) | copy-start | bytes 6291460
  52.1 99.3 %all-to-all-start = ((bf16[256,8,1024]{2,0,1:T(8,128)(2,1)}), bf16[256,8,1024]{2,0,1:T(8,128)(2,1)}, u32[]{:S(2)}, u32[]{:S(2)}) async-start(bf16[256,8,1024]{2,0,1:T(8,128)(2,1)} %bitcast.12), calls=%async_computation | async-start | bytes 8388608 | tf_op jit(solution)/shard_map/all_to_all | solution.py:14
  57.8 37.9 %all-gather.5.cloned.1.call-start = ((), (), s32[]{:S(2)}) async-start(), calls=%async_computation.3 | async-start | bytes 5242880 | tf_op jit(solution)/shard_map/all_gather | solution.py:12
  59.0 169.9 %reduce-scatter.2.cloned.1.call-start = ((), (), s32[]{:S(2)}) async-start(), calls=%async_computation.4 | async-start | bytes 2359296 | tf_op jit(solution)/shard_map/reduce_scatter | solution.py:21
  228.8 4.8 %copy-start = (bf16[1024,2048]{1,0:T(8,128)(2,1)S(1)}, bf16[1024,2048]{1,0:T(8,128)(2,1)}, u32[]{:S(2)}) copy-start(bf16[1024,2048]{1,0:T(8,128)(2,1)} %all-gather.5.cloned.1.call-done) | copy-start | bytes 12582916
Sparse Core Ops, SparseCore 0:
  10.1 37.1 all-gather.2
  60.7 34.9 all-gather.4
  161.6 67.2 reduce-scatter.1
where the time goes:
time: 243 us; the launch traced here: 242 us
  waiting for transfers between devices  195 us (80%)
  between operations  13.8 us (6%)
  local copies, waits for them, and re-layouts  11.7 us (5%)
  matrix products  9.92 us (4%)
  other arithmetic  5.93 us (2%)
  starting transfers between devices  5.77 us (2%)
    reduce_scatter x1, waiting for transfers between devices, per_device(): lax.psum_scatter(lax.dot_general(down_columns, hidden, (((0,), (1,)), (()...  67.4 us
    all_to_all x1, waiting for transfers between devices, per_device(): lax.all_to_all(up_columns, 'fs', split_axis=1, concat_axis=0, tiled=True)  55.8 us
    all_gather x1, waiting for transfers between devices, per_device(): lax.all_gather(up_scaled, ('gr', 'tp'), axis=1, tiled=True)  37.3 us
    all_gather x1, waiting for transfers between devices, per_device(): lax.all_gather(down_half, ('gr', 'tp'), axis=1, tiled=True)  34.6 us
    dot_general x1, matrix products, per_device(): lax.dot_general(down_columns, hidden, (((0,), (1,)), ((), ())), preferred...  9.92 us
    unnamed x6, local copies, waits for them, and re-layouts  6.83 us
    all_to_all x1, starting transfers between devices, per_device(): lax.all_to_all(up_columns, 'fs', split_axis=1, concat_axis=0, tiled=True)  5.65 us
  transfers between devices with their start and end apart: 4, of which 4 were waited for; matrix products, arithmetic and copies ran while one was open for 1% of the time, Pallas kernels for 0%

commit v1 on v0

--- a/solution.py
+++ b/solution.py
@@ -2,6 +2,8 @@
 import jax.numpy as jnp
 from jax import lax
 from jax.sharding import PartitionSpec as P
+
+attach_sample_by_axis = lambda a0, dim_k: jnp.concatenate(lax.all_gather(a0, ("gr", "tp")), dim_k)
 
 
 def per_device(tokens, norm_gain, up_weight, down_weight):
@@ -9,7 +11,7 @@
     down_half = down_weight.astype(jnp.bfloat16)
     up_columns, down_columns = (
         lax.all_gather(up_scaled, ("gr", "tp"), axis=1, tiled=True),
-        lax.all_gather(down_half, ("gr", "tp"), axis=1, tiled=True),
+        attach_sample_by_axis(down_half, 1),
     )
     up_block = lax.all_to_all(up_columns, "fs", split_axis=1, concat_axis=0, tiled=True)
     widened = tokens.astype(jnp.float32)

time: 243 us -> 240 us (0.988)
  waiting for transfers between devices: 195 us -> 186 us
  local copies, waits for them, and re-layouts: 11.7 us -> 18.3 us
    all_to_all x1, waiting for transfers between devices: 55.8 us -> 46.9 us  [per_device(): lax.all_to_all(up_columns, 'fs', split_axis=1, concat_axis=0, tiled=True)]
    all_gather x0 -> x1, local copies, waits for them, and re-layouts: none -> 5.42 us  [lax.all_gather(a0, ('gr', 'tp'))]
  transfers between devices with their start and end apart: 4 -> 4, of which waited for: 4 -> 4; matrix products, arithmetic and copies ran while one was open for 1% -> 5% of each run, Pallas kernels for 0% -> 0%
where the time goes in v1:
time: 240 us; the launch traced here: 239 us
  waiting for transfers between devices  186 us (78%)
  local copies, waits for them, and re-layouts  18.3 us (8%)
  between operations  13.8 us (6%)
  matrix products  9.33 us (4%)
  other arithmetic  5.93 us (2%)
  starting transfers between devices  5.77 us (2%)
    reduce_scatter x1, waiting for transfers between devices, per_device(): lax.psum_scatter(lax.dot_general(down_columns, hidden, (((0,), (1,)), (()...  67.1 us
    all_to_all x1, waiting for transfers between devices, per_device(): lax.all_to_all(up_columns, 'fs', split_axis=1, concat_axis=0, tiled=True)  46.9 us
    all_gather x1, waiting for transfers between devices, per_device(): lax.all_gather(up_scaled, ('gr', 'tp'), axis=1, tiled=True)  37.3 us
    all_gather x1, waiting for transfers between devices, lax.all_gather(a0, ('gr', 'tp'))  34.6 us
    dot_general x1, matrix products, per_device(): lax.dot_general(down_columns, hidden, (((0,), (1,)), ((), ())), preferred...  9.33 us
    unnamed x6, local copies, waits for them, and re-layouts  8.06 us
    all_to_all x1, starting transfers between devices, per_device(): lax.all_to_all(up_columns, 'fs', split_axis=1, concat_axis=0, tiled=True)  5.65 us
    all_gather x1, local copies, waits for them, and re-layouts, lax.all_gather(a0, ('gr', 'tp'))  5.42 us
  transfers between devices with their start and end apart: 4, of which 4 were waited for; matrix products, arithmetic and copies ran while one was open for 5% of the time, Pallas kernels for 0%

profile of v1, /device:TPU:0, one launch (start us, length us, event | category | flops | bytes accessed | tf_op | source)
XLA Modules:
  0.0 239.1 jit_solution(3171602579456428717)
XLA Ops:
  7.2 0.0 all-gather.4.cloned.1.call-start
  7.2 2.7 %multiply_convert_fusion.1 = bf16[256,2048]{1,0:T(8,128)(2,1)} fusion(f32[256,2048]{1,0:T(8,128)} %param.6, f32[256]{0:T(256)} %param.5), kind=kLoop, calls=%fused_computation.10 | loop fusion | flops 1048576 | bytes 3146752 | tf_op jit(solution)/shard_map/convert_element_type | solution.py:10
  10.0 0.0 all-gather.4.cloned.1.call-update
  10.0 37.3 %all-gather.4.cloned.1.call-done = bf16[256,8192]{1,0:T(8,128)(2,1)} async-done(((bf16[256,2048]{1,0:T(8,128)(2,1)}), bf16[256,8192]{1,0:T(8,128)(2,1)}) %all-gather.4.cloned.1.call-update) | async-done | bytes 4194320 | tf_op jit(solution)/shard_map/all_gather | solution.py:13
  47.3 4.8 %copy.12 = bf16[32,8,8,1024]{3,2,0,1:T(8,128)(2,1)} copy(bf16[32,8,8,1024]{3,2,1,0:T(8,128)(2,1)} %bitcast.21) | data formatting | bytes 8388608 | tf_op jit(solution)/shard_map/all_to_all | solution.py:16
  52.1 0.0 copy-start
  52.1 5.6 %all-to-all-start = ((bf16[256,8,1024]{2,0,1:T(8,128)(2,1)}), bf16[256,8,1024]{2,0,1:T(8,128)(2,1)}, u32[]{:S(2)}, u32[]{:S(2)}) async-start(bf16[256,8,1024]{2,0,1:T(8,128)(2,1)} %bitcast.16), calls=%async_computation | async-start | bytes 8388608 | tf_op jit(solution)/shard_map/all_to_all | solution.py:16
  57.8 0.0 all-gather.6.cloned.1.call-start
  57.8 0.0 copy-done
  57.9 1.1 convert_element_type.22
  59.0 0.0 all-gather.6.cloned.1.call-update
  59.0 0.0 reduce-scatter.2.cloned.1.call-start
  59.0 2.1 fusion
  61.1 34.6 %all-gather.6.cloned.1.call-done = bf16[4096,512]{1,0:T(8,128)(2,1)} async-done(((bf16[1024,512]{1,0:T(8,128)(2,1)}), bf16[4096,512]{1,0:T(8,128)(2,1)}) %all-gather.6.cloned.1.call-update) | async-done | bytes 4194320 | tf_op jit(solution)/shard_map/all_gather | solution.py:6
  95.7 5.4 %copy.8 = bf16[4,1024,512]{2,0,1:T(4,128)(2,1)S(1)} copy(bf16[4,1024,512]{2,1,0:T(8,128)(2,1)} %bitcast.20) | data formatting | bytes 8388608 | tf_op jit(solution)/shard_map/all_gather | solution.py:6
  101.1 0.0 copy-start.1
  101.1 3.4 %copy.10 = bf16[128,8,4,512]{3,1,2,0:T(8,128)(2,1)} copy(bf16[128,8,4,512]{3,2,1,0:T(4,128)(2,1)S(1)} %bitcast.17) | data formatting | bytes 8388608
  104.6 46.9 %all-to-all-done = bf16[256,8,1024]{2,0,1:T(8,128)(2,1)} async-done(((bf16[256,8,1024]{2,0,1:T(8,128)(2,1)}), bf16[256,8,1024]{2,0,1:T(8,128)(2,1)}, u32[]{:S(2)}, u32[]{:S(2)}) %all-to-all-start) | async-done | bytes 4194336 | tf_op jit(solution)/shard_map/all_to_all | solution.py:16
  151.5 0.0 copy-done.1
  151.5 9.3 %fusion.2 = bf16[2048,512]{0,1:T(8,128)(2,1)} fusion(bf16[1024,2048]{1,0:T(8,128)(2,1)} %bitcast.18, bf16[2048,1024]{1,0:T(8,128)(2,1)} %bitcast.1, bf16[512,2048]{1,0:T(8,128)(2,1)S(1)} %copy-done.1, f32[512]{0:T(512)S(1)} %add_rsqrt_fusion), kind=kOutput, calls=%fused_computation.6 | convolution fusion | flops 4300734464 | bytes 12584960 | tf_op jit(solution)/shard_map/dot_general | solution.py:24
  160.8 0.0 reduce-scatter.2.cloned.1.call-update
  160.8 67.1 %reduce-scatter.2.cloned.1.call-done = bf16[256,512]{0,1:T(8,128)(2,1)} async-done(((bf16[2048,512]{0,1:T(8,128)(2,1)}), bf16[256,512]{0,1:T(8,128)(2,1)}) %reduce-scatter.2.cloned.1.call-update) | async-done | bytes 262160 | tf_op jit(solution)/shard_map/reduce_scatter | solution.py:23
  228.0 4.6 %copy.14 = bf16[2048,1024]{1,0:T(8,128)(2,1)} copy(bf16[2048,1024]{1,0:T(8,128)(2,1)} %bitcast.1) | data formatting | bytes 8388608
  (1 shorter events, 0.0 us)
Async XLA Ops:
  7.2 40.2 %all-gather.4.cloned.1.call-start = ((), (), s32[]{:S(2)}) async-start(), calls=%async_computation.2 | async-start | bytes 5242880 | tf_op jit(solution)/shard_map/all_gather | solution.py:13
  52.1 5.7 %copy-start = (f32[1024,512]{1,0:T(8,128)S(1)}, f32[1024,512]{1,0:T(8,128)}, u32[]{:S(2)}) copy-start(f32[1024,512]{1,0:T(8,128)} %param.7) | copy-start | bytes 6291460
  52.1 99.3 %all-to-all-start = ((bf16[256,8,1024]{2,0,1:T(8,128)(2,1)}), bf16[256,8,1024]{2,0,1:T(8,128)(2,1)}, u32[]{:S(2)}, u32[]{:S(2)}) async-start(bf16[256,8,1024]{2,0,1:T(8,128)(2,1)} %bitcast.16), calls=%async_computation | async-start | bytes 8388608 | tf_op jit(solution)/shard_map/all_to_all | solution.py:16
  57.8 37.9 %all-gather.6.cloned.1.call-start = ((), (), s32[]{:S(2)}) async-start(), calls=%async_computation.4 | async-start | bytes 5242880 | tf_op jit(solution)/shard_map/all_gather | solution.py:6
  59.0 169.0 %reduce-scatter.2.cloned.1.call-start = ((), (), s32[]{:S(2)}) async-start(), calls=%async_computation.3 | async-start | bytes 2359296 | tf_op jit(solution)/shard_map/reduce_scatter | solution.py:23
  101.1 50.4 %copy-start.1 = (bf16[512,2048]{1,0:T(8,128)(2,1)S(1)}, bf16[512,2048]{1,0:T(8,128)(2,1)}, u32[]{:S(2)}) copy-start(bf16[512,2048]{1,0:T(8,128)(2,1)} %param.4) | copy-start | bytes 6291460
Sparse Core Ops, SparseCore 0:
  10.1 37.1 all-gather.3
  60.7 34.9 all-gather.5
  161.0 66.9 reduce-scatter.1
